TPU v7x, 32 devices: a whole 2x2x4 slice. The times are simulated.
32 devices in a mesh: fs: 4 (over y, x), tp: 8 (over z, core).
Axes of the slice: x: 2, y: 2, z: 4, core: 2. Of those that a mesh axis runs over, the one named last changes fastest.
Arguments:
- prompt: bfloat16 [4096, 2048], P(('fs', 'tp')), may hold values from -6 to 6
- norm_gain: float32 [2048], P('tp'), may hold values from 0.1 to 1.9
- gate_master: float32 [8, 2, 512, 2048], P(None, None, 'fs', 'tp'), may hold values from -0.125 to 0.125
- up_master: float32 [8, 2, 512, 2048], P(None, None, 'fs', 'tp'), may hold values from -0.125 to 0.125
- down_master: float32 [8, 2, 512, 2048], P(None, None, 'fs', 'tp'), may hold values from -0.25 to 0.25
- group_pick: int32 [4096, 1], P(('fs', 'tp')), may hold values from 0 to 7; in each aligned block of 128 rows (0 to 127, 128 to 255, ...) at most 32 rows name the same one
- route_weight: bfloat16 [4096, 2], P(('fs', 'tp')), may hold values from 0.099609375 to 1
Outputs:
- gate_serve: bfloat16 [8, 2, 512, 2048], P('tp', None, 'fs')
- up_serve: bfloat16 [8, 2, 512, 2048], P('tp', None, 'fs')
- down_serve: bfloat16 [8, 2, 512, 2048], P('tp', None, 'fs')
- mixed: bfloat16 [4096, 2048], P(('fs', 'tp'))
Inputs may be any that keep to these rules, and one draw needn't show every extreme that they name: `group_pick`: in the rows of one device no group is named by more than 32 rows, and in every draw some device's rows name one group exactly 32 times.
All inputs are finite; a program needn't handle non-finite values.
Results may differ from a plain program's by a relative error of at most 0.0081.
Values may be sent and summed in bfloat16 or wider, within the bound.
A program may use at most 64 MiB of HBM per device.

v0:
```python
import jax
import jax.numpy as jnp
from jax import lax
from jax.sharding import PartitionSpec as P

EPS = 1e-06


def expert_rows(group_rows, weights, pieces):
    gate_piece, up_piece, down_piece = pieces
    expert_count = gate_piece.shape[1]
    unit_count = gate_piece.shape[2]
    model_width = gate_piece.shape[3]
    row_count = group_rows.shape[0]
    gate_matrix = gate_piece.reshape(expert_count * unit_count, model_width)
    up_matrix = up_piece.reshape(expert_count * unit_count, model_width)
    down_matrix = down_piece.reshape(expert_count * unit_count, model_width)
    gate_pre = jnp.einsum("sd,hd->sh", group_rows, gate_matrix, preferred_element_type=jnp.float32)
    up_pre = jnp.einsum("sd,hd->sh", group_rows, up_matrix, preferred_element_type=jnp.float32)
    active = (jax.nn.silu(gate_pre) * up_pre).reshape(row_count, expert_count, unit_count)
    hidden = (weights.astype(jnp.float32)[:, :, None] * active).reshape(
        row_count, expert_count * unit_count
    )
    hidden = hidden.astype(jnp.bfloat16)
    return jnp.dot(hidden, down_matrix, preferred_element_type=jnp.float32)


def per_device(prompt, norm_gain, gate_master, up_master, down_master, group_pick, route_weight):
    group_total = lax.axis_size("tp")
    gate_local = (gate_master * norm_gain).astype(jnp.bfloat16)
    up_local = (up_master * norm_gain).astype(jnp.bfloat16)
    down_local = down_master.astype(jnp.bfloat16)
    gate_serve, up_serve, down_serve = (
        lax.all_to_all(gate_local, "tp", split_axis=0, concat_axis=3, tiled=True),
        lax.all_to_all(up_local, "tp", split_axis=0, concat_axis=3, tiled=True),
        lax.all_to_all(down_local, "tp", split_axis=0, concat_axis=3, tiled=True),
    )
    values = prompt.astype(jnp.float32)
    normed = (values * lax.rsqrt(jnp.mean(values * values, axis=1, keepdims=True) + EPS)).astype(
        jnp.bfloat16
    )
    tok_count = prompt.shape[0]
    capacity = 2 * tok_count // group_total
    slot_total = group_total * capacity
    chosen = group_pick[:, 0]
    member = (chosen[:, None] == jnp.arange(group_total, dtype=jnp.int32)[None, :]).astype(
        jnp.int32
    )
    slot_rank = jnp.sum(jnp.cumsum(member, axis=0) * member, axis=1) - 1
    target = chosen * capacity + slot_rank
    placing = (jnp.arange(slot_total, dtype=jnp.int32)[:, None] == target[None, :]).astype(
        jnp.bfloat16
    )
    send_rows = jnp.dot(placing, normed, preferred_element_type=jnp.float32).astype(jnp.bfloat16)
    send_weights = jnp.dot(placing, route_weight, preferred_element_type=jnp.float32).astype(
        jnp.bfloat16
    )
    got_rows, got_weights = (
        lax.all_to_all(
            send_rows.reshape(group_total, capacity, -1),
            "tp",
            split_axis=0,
            concat_axis=0,
            tiled=True,
        ),
        lax.all_to_all(
            send_weights.reshape(group_total, capacity, -1),
            "tp",
            split_axis=0,
            concat_axis=0,
            tiled=True,
        ),
    )
    group_rows = got_rows.reshape(slot_total, -1)
    weights = got_weights.reshape(slot_total, -1)
    gathered = (
        lax.all_gather(gate_serve, "fs", axis=2, tiled=True),
        lax.all_gather(up_serve, "fs", axis=2, tiled=True),
        lax.all_gather(down_serve, "fs", axis=2, tiled=True),
    )
    summed = expert_rows(group_rows, weights, gathered)
    result = summed.astype(jnp.bfloat16).reshape(group_total, capacity, -1)
    returned = lax.all_to_all(result, "tp", split_axis=0, concat_axis=0, tiled=True)
    mixed = jnp.einsum(
        "st,sd->td", placing, returned.reshape(slot_total, -1), preferred_element_type=jnp.float32
    ).astype(jnp.bfloat16)
    return (gate_serve, up_serve, down_serve, mixed)


def solution(mesh):
    placed = (
        P(("fs", "tp"), None),
        P("tp"),
        P(None, None, "fs", "tp"),
        P(None, None, "fs", "tp"),
        P(None, None, "fs", "tp"),
        P(("fs", "tp"), None),
        P(("fs", "tp"), None),
    )
    return jax.shard_map(
        per_device,
        mesh=mesh,
        in_specs=placed,
        out_specs=(
            P("tp", None, "fs", None),
            P("tp", None, "fs", None),
            P("tp", None, "fs", None),
            P(("fs", "tp"), None),
        ),
        check_vma=False,
    )
```

profile of v0, /device:TPU:0, one launch (start us, length us, event | category | flops | bytes accessed | tf_op | source)
XLA Modules:
  0.0 250.6 jit_solution(5716967491578532564)
XLA Ops:
  7.2 0.0 all-gather.4.cloned.1.call-start
  7.2 2.7 %multiply_convert_fusion = (bf16[8,2,128,256]{3,2,1,0:T(8,128)(2,1)S(1)}, bf16[8,2,128,256]{3,2,1,0:T(8,128)(2,1)S(1)}) fusion(f32[8,2,128,256]{3,2,1,0:T(8,128)} %param.10, f32[256]{0:T(256)} %param.8, f32[8,2,128,256]{3,2,1,0:T(8,128)} %param.9), kind=kLoop, calls=%fused_computation.3 | loop fusion | flops 2097152 | bytes 6292480 | tf_op jit(solution)/shard_map/convert_element_type | solution.py:31
  9.9 32.7 %all_to_all.69 = bf16[8,2,128,256]{3,2,1,0:T(8,128)(2,1)S(1)} all-to-all(bf16[8,2,128,256]{3,2,1,0:T(8,128)(2,1)S(1)} %get-tuple-element.5), channel_id=1, replica_groups=mesh['fs'=4,'tp'=8] {'tp'}, dimensions={0} | all-to-all | bytes 2097152 | tf_op jit(solution)/shard_map/all_to_all | solution.py:34
  42.7 1.1 copy.32
  43.8 0.0 all-gather.6.cloned.1.call-start
  43.8 29.0 %all_to_all.70 = bf16[8,2,128,256]{3,2,1,0:T(8,128)(2,1)S(1)} all-to-all(bf16[8,2,128,256]{3,2,1,0:T(8,128)(2,1)S(1)} %get-tuple-element.4), channel_id=1, replica_groups=mesh['fs'=4,'tp'=8] {'tp'}, dimensions={0} | all-to-all | bytes 2097152 | tf_op jit(solution)/shard_map/all_to_all | solution.py:35
  72.8 1.1 copy.33
  74.0 0.0 all-gather.8.cloned.1.call-start
  74.0 0.1 convert_element_type.46
  74.2 29.0 %all_to_all.71 = bf16[8,2,128,256]{3,2,1,0:T(8,128)(2,1)S(1)} all-to-all(bf16[8,2,128,256]{3,2,1,0:T(8,128)(2,1)S(1)} %convert_element_type.46), channel_id=1, replica_groups=mesh['fs'=4,'tp'=8] {'tp'}, dimensions={0} | all-to-all | bytes 2097152 | tf_op jit(solution)/shard_map/all_to_all | solution.py:36
  103.1 1.1 copy.34
  104.3 0.1 fusion.10
  104.4 0.2 reduce_window_sum.11
  104.5 0.2 select_reduce_fusion
  104.7 0.1 convolution_convert_fusion.3
  104.9 0.1 reshape.61
  105.0 0.6 copy.28
  105.6 3.3 %all-to-all-start.3 = ((bf16[8,32,2]{1,2,0:T(2,128)(2,1)}), bf16[8,32,2]{1,2,0:T(2,128)(2,1)S(1)}, u32[]{:S(2)}, u32[]{:S(2)}) async-start(bf16[8,32,2]{1,2,0:T(2,128)(2,1)} %copy.28), calls=%async_computation.3 | async-start | bytes 8192 | tf_op jit(solution)/shard_map/all_to_all | solution.py:66
  108.9 0.2 fusion.2
  109.1 1.6 convolution_convert_fusion
  110.7 3.7 %all-to-all-done.3 = bf16[8,32,2]{1,2,0:T(2,128)(2,1)S(1)} async-done(((bf16[8,32,2]{1,2,0:T(2,128)(2,1)}), bf16[8,32,2]{1,2,0:T(2,128)(2,1)S(1)}, u32[]{:S(2)}, u32[]{:S(2)}) %all-to-all-start.3) | async-done | bytes 1056 | tf_op jit(solution)/shard_map/all_to_all | solution.py:66
  114.3 3.6 %all-to-all-start.4 = ((bf16[8,32,2048]{2,1,0:T(8,128)(2,1)}), bf16[8,32,2048]{2,1,0:T(8,128)(2,1)S(1)}, u32[]{:S(2)}, u32[]{:S(2)}) async-start(bf16[8,32,2048]{2,1,0:T(8,128)(2,1)} %bitcast.8), calls=%async_computation.4 | async-start | bytes 2097152 | tf_op jit(solution)/shard_map/all_to_all | solution.py:59
  117.9 0.1 copy.31
  118.0 0.3 mul.62
  118.4 0.2 copy.35
  118.6 25.8 %all-to-all-done.4 = bf16[8,32,2048]{2,1,0:T(8,128)(2,1)S(1)} async-done(((bf16[8,32,2048]{2,1,0:T(8,128)(2,1)}), bf16[8,32,2048]{2,1,0:T(8,128)(2,1)S(1)}, u32[]{:S(2)}, u32[]{:S(2)}) %all-to-all-start.4) | async-done | bytes 1048608 | tf_op jit(solution)/shard_map/all_to_all | solution.py:59
  144.4 4.6 %fusion.12 = f32[256,1024]{1,0:T(8,128)} fusion(bf16[256,2048]{1,0:T(8,128)(2,1)S(1)} %bitcast.47, bf16[1024,2048]{1,0:T(8,128)(2,1)} %bitcast.54), kind=kOutput, calls=%fused_computation.26 | convolution fusion | flops 1073741824 | bytes 6291456 | tf_op jit(solution)/shard_map/sd,hd->sh/dot_general | solution.py:18
  149.0 1.4 all-gather.6.cloned.1.call-done
  150.5 55.0 %all-gather.8.cloned.1.call-done = bf16[1,2,512,2048]{3,2,1,0:T(8,128)(2,1)} async-done(((bf16[1,2,128,2048]{3,2,1,0:T(8,128)(2,1)}), bf16[1,2,512,2048]{3,2,1,0:T(8,128)(2,1)}) %all-gather.8.cloned.1.call-update) | async-done | bytes 4194320 | tf_op jit(solution)/shard_map/all_gather | solution.py:79
  205.5 6.4 %convolution_convert_fusion.1 = bf16[256,2048]{1,0:T(8,128)(2,1)S(1)} fusion(bf16[1024,2048]{1,0:T(8,128)(2,1)} %bitcast.56, f32[256,1024]{1,0:T(8,128)S(1)} %bitcast.49, bf16[256,2048]{1,0:T(8,128)(2,1)S(1)} %bitcast.48, bf16[1024,2048]{1,0:T(8,128)(2,1)} %bitcast.55, f32[256,1024]{1,0:T(8,128)} %fusion.12), kind=kOutput, calls=%fused_computation.1 | convolution fusion | flops 2149842944 | bytes 12582912 | tf_op jit(solution)/shard_map/dot_general | solution.py:25
  211.9 31.0 %all_to_all.72 = bf16[8,32,2048]{2,1,0:T(8,128)(2,1)S(1)} all-to-all(bf16[8,32,2048]{2,1,0:T(8,128)(2,1)S(1)} %bitcast.50), channel_id=1, replica_groups=mesh['fs'=4,'tp'=8] {'tp'}, dimensions={0} | all-to-all | bytes 2097152 | tf_op jit(solution)/shard_map/all_to_all | solution.py:83
  242.9 1.1 convolution_convert_fusion.2
  (15 shorter events, 0.1 us)
Async XLA Ops:
  7.2 97.6 %copy-start = (bf16[128,2]{0,1:T(2,128)(2,1)S(1)}, bf16[128,2]{0,1:T(2,128)(2,1)}, u32[]{:S(2)}) copy-start(bf16[128,2]{0,1:T(2,128)(2,1)} %param.13) | copy-start | bytes 1540
  7.2 137.2 %all-gather.4.cloned.1.call-start = ((), (), s32[]{:S(2)}) async-start(), calls=%async_computation.6 | async-start | bytes 5242880 | tf_op jit(solution)/shard_map/all_gather | solution.py:77
  42.7 31.4 %copy-start.1 = (f32[8,2,128,256]{3,2,1,0:T(8,128)S(1)}, f32[8,2,128,256]{3,2,1,0:T(8,128)}, u32[]{:S(2)}) copy-start(f32[8,2,128,256]{3,2,1,0:T(8,128)} %param.11) | copy-start | bytes 6291460
  43.8 106.7 %all-gather.6.cloned.1.call-start = ((), (), s32[]{:S(2)}) async-start(), calls=%async_computation.7 | async-start | bytes 5242880 | tf_op jit(solution)/shard_map/all_gather | solution.py:78
  73.9 30.3 %copy-start.3 = (s32[128,1]{0,1:T(1,128)S(1)}, s32[128,1]{0,1:T(1,128)}, u32[]{:S(2)}) copy-start(s32[128,1]{0,1:T(1,128)} %param.12) | copy-start | bytes 1540
  73.9 35.0 %copy-start.2 = (bf16[128,2048]{1,0:T(8,128)(2,1)S(1)}, bf16[128,2048]{1,0:T(8,128)(2,1)}, u32[]{:S(2)}) copy-start(bf16[128,2048]{1,0:T(8,128)(2,1)} %param.7) | copy-start | bytes 1572868
  74.0 131.5 %all-gather.8.cloned.1.call-start = ((), (), s32[]{:S(2)}) async-start(), calls=%async_computation.8 | async-start | bytes 5242880 | tf_op jit(solution)/shard_map/all_gather | solution.py:79
  105.6 8.8 %all-to-all-start.3 = ((bf16[8,32,2]{1,2,0:T(2,128)(2,1)}), bf16[8,32,2]{1,2,0:T(2,128)(2,1)S(1)}, u32[]{:S(2)}, u32[]{:S(2)}) async-start(bf16[8,32,2]{1,2,0:T(2,128)(2,1)} %copy.28), calls=%async_computation.3 | async-start | bytes 8192 | tf_op jit(solution)/shard_map/all_to_all | solution.py:66
  114.3 30.1 %all-to-all-start.4 = ((bf16[8,32,2048]{2,1,0:T(8,128)(2,1)}), bf16[8,32,2048]{2,1,0:T(8,128)(2,1)S(1)}, u32[]{:S(2)}, u32[]{:S(2)}) async-start(bf16[8,32,2048]{2,1,0:T(8,128)(2,1)} %bitcast.8), calls=%async_computation.4 | async-start | bytes 2097152 | tf_op jit(solution)/shard_map/all_to_all | solution.py:59
Sparse Core Ops, SparseCore 0:
  43.9 51.4 all-gather.3
  97.9 52.5 all-gather.5
  152.9 52.5 all-gather.7
where the time goes:
time: 251 us
  blocking collectives  122 us (49%)
  waiting for transfers between devices  86 us (34%)
  matrix products  13.9 us (6%)
  between operations  13.9 us (6%)
  starting transfers between devices  6.99 us (3%)
  local copies, waits for them, and re-layouts  4.69 us (2%)
  other arithmetic  3.46 us (1%)
    all_gather x1, waiting for transfers between devices, per_device(): lax.all_gather(down_serve, 'fs', axis=2, tiled=True)  55 us
    all_to_all x1, blocking collectives, per_device(): lax.all_to_all(gate_local, 'tp', split_axis=0, concat_axis=3, tiled=True)  32.7 us
    all_to_all x1, blocking collectives, per_device(): lax.all_to_all(result, 'tp', split_axis=0, concat_axis=0, tiled=True)  31 us
    all_to_all x1, blocking collectives, per_device(): lax.all_to_all(up_local, 'tp', split_axis=0, concat_axis=3, tiled=True)  29 us
    all_to_all x1, blocking collectives, per_device(): lax.all_to_all(down_local, 'tp', split_axis=0, concat_axis=3, tiled=True)  29 us
    all_to_all x1, waiting for transfers between devices, per_device(): lax.all_to_all(send_rows.reshape(group_total, capacity, -1), 'tp', split_...  25.8 us
    dot_general x1, matrix products, expert_rows(): return jnp.dot(hidden, down_matrix, preferred_element_type=jnp.float32)  6.42 us
  transfers between devices with their start and end apart: 5, of which 4 were waited for; matrix products, arithmetic and copies ran while one was open for 4% of the time, Pallas kernels for 0%

commit v1 on v0

--- a/solution.py
+++ b/solution.py
@@ -76,7 +76,7 @@
     gathered = (
         lax.all_gather(gate_serve, "fs", axis=2, tiled=True),
         lax.all_gather(up_serve, "fs", axis=2, tiled=True),
-        lax.all_gather(down_serve, "fs", axis=2, tiled=True),
+        jnp.concatenate(lax.all_gather(down_serve, "fs"), axis=2),
     )
     summed = expert_rows(group_rows, weights, gathered)
     result = summed.astype(jnp.bfloat16).reshape(group_total, capacity, -1)

time: 251 us -> 252 us (level)
  blocking collectives: 122 us -> 90.7 us
  waiting for transfers between devices: 86 us -> 104 us
  local copies, waits for them, and re-layouts: 4.69 us -> 12.8 us
  starting transfers between devices: 6.99 us -> 11.6 us
    all_gather x1, waiting for transfers between devices: 55 us -> 0.02 us  [per_device(): lax.all_gather(down_serve, 'fs')]
    all_gather x1, waiting for transfers between devices: 1.44 us -> 50.6 us  [per_device(): lax.all_gather(up_serve, 'fs', axis=2, tiled=True)]
    all_to_all x1 -> x0, blocking collectives: 31 us -> none  [per_device(): lax.all_to_all(result, 'tp', split_axis=0, concat_axis=0, tiled=True)]
    all_to_all x0 -> x1, waiting for transfers between devices: none -> 25.3 us  [per_device(): lax.all_to_all(result, 'tp', split_axis=0, concat_axis=0, tiled=True)]
    all_gather x0 -> x2, local copies, waits for them, and re-layouts: none -> 6.05 us  [per_device(): lax.all_gather(down_serve, 'fs')]
    all_to_all x1, waiting for transfers between devices: 25.8 us -> 21 us  [per_device(): lax.all_to_all(send_rows.reshape(group_total, capacity, -1), 'tp', split_...]
    all_to_all x0 -> x1, starting transfers between devices: none -> 4.6 us  [per_device(): lax.all_to_all(result, 'tp', split_axis=0, concat_axis=0, tiled=True)]
    all_to_all x1, blocking collectives: 29 us -> 32.7 us  [per_device(): lax.all_to_all(down_local, 'tp', split_axis=0, concat_axis=3, tiled=True)]
  transfers between devices with their start and end apart: 5 -> 6, of which waited for: 4 -> 5; matrix products, arithmetic and copies ran while one was open for 4% -> 8% of each run, Pallas kernels for 0% -> 0%
where the time goes in v1:
time: 252 us; the launch traced here: 251 us
  waiting for transfers between devices  104 us (41%)
  blocking collectives  90.7 us (36%)
  matrix products  14.5 us (6%)
  between operations  13.9 us (6%)
  local copies, waits for them, and re-layouts  12.8 us (5%)
  starting transfers between devices  11.6 us (5%)
  other arithmetic  3.27 us (1%)
    all_gather x1, waiting for transfers between devices, per_device(): lax.all_gather(up_serve, 'fs', axis=2, tiled=True)  50.6 us
    all_to_all x1, blocking collectives, per_device(): lax.all_to_all(down_local, 'tp', split_axis=0, concat_axis=3, tiled=True)  32.7 us
    all_to_all x1, blocking collectives, per_device(): lax.all_to_all(up_local, 'tp', split_axis=0, concat_axis=3, tiled=True)  29 us
    all_to_all x1, blocking collectives, per_device(): lax.all_to_all(gate_local, 'tp', split_axis=0, concat_axis=3, tiled=True)  29 us
    all_to_all x1, waiting for transfers between devices, per_device(): lax.all_to_all(result, 'tp', split_axis=0, concat_axis=0, tiled=True)  25.3 us
    all_to_all x1, waiting for transfers between devices, per_device(): lax.all_to_all(send_rows.reshape(group_total, capacity, -1), 'tp', split_...  21 us
    dot_general x1, matrix products, expert_rows(): return jnp.dot(hidden, down_matrix, preferred_element_type=jnp.float32)  7.29 us
    all_gather x2, local copies, waits for them, and re-layouts, per_device(): lax.all_gather(down_serve, 'fs')  6.05 us
  transfers between devices with their start and end apart: 6, of which 5 were waited for; matrix products, arithmetic and copies ran while one was open for 8% of the time, Pallas kernels for 0%

profile of v1, /device:TPU:0, one launch (start us, length us, event | category | flops | bytes accessed | tf_op | source)
XLA Modules:
  0.0 251.1 jit_solution(1728597082328522545)
XLA Ops:
  7.2 1.8 copy.41
  9.1 32.7 %all_to_all.69 = bf16[8,2,128,256]{2,3,1,0:T(8,128)(2,1)S(1)} all-to-all(bf16[8,2,128,256]{2,3,1,0:T(8,128)(2,1)S(1)} %copy.41), channel_id=1, replica_groups=mesh['fs'=4,'tp'=8] {'tp'}, dimensions={0} | all-to-all | bytes 2097152 | tf_op jit(solution)/shard_map/all_to_all | solution.py:36
  41.9 1.3 copy.46
  43.3 2.6 %multiply_convert_fusion = (bf16[8,2,128,256]{3,2,1,0:T(8,128)(2,1)S(1)}, bf16[8,2,128,256]{3,2,1,0:T(8,128)(2,1)S(1)}) fusion(f32[8,2,128,256]{3,2,1,0:T(8,128)} %param.10, f32[256]{0:T(256)S(1)} %copy-done.3, f32[8,2,128,256]{3,2,1,0:T(8,128)} %param.9), kind=kLoop, calls=%fused_computation.3 | loop fusion | flops 2097152 | bytes 6292480 | tf_op jit(solution)/shard_map/convert_element_type | solution.py:31
  45.9 29.0 %all_to_all.70 = bf16[8,2,128,256]{3,2,1,0:T(8,128)(2,1)S(1)} all-to-all(bf16[8,2,128,256]{3,2,1,0:T(8,128)(2,1)S(1)} %get-tuple-element.21), channel_id=1, replica_groups=mesh['fs'=4,'tp'=8] {'tp'}, dimensions={0} | all-to-all | bytes 2097152 | tf_op jit(solution)/shard_map/all_to_all | solution.py:34
  74.9 1.1 copy.50
  76.1 29.0 %all_to_all.71 = bf16[8,2,128,256]{3,2,1,0:T(8,128)(2,1)S(1)} all-to-all(bf16[8,2,128,256]{3,2,1,0:T(8,128)(2,1)S(1)} %get-tuple-element.20), channel_id=1, replica_groups=mesh['fs'=4,'tp'=8] {'tp'}, dimensions={0} | all-to-all | bytes 2097152 | tf_op jit(solution)/shard_map/all_to_all | solution.py:35
  105.1 1.1 copy.51
  106.2 0.1 fusion.10
  106.3 0.2 reduce_window_sum.11
  106.5 0.2 select_reduce_fusion
  106.7 0.1 convolution_convert_fusion.3
  106.8 0.1 reshape.62
  106.9 0.6 copy.43
  107.5 3.3 %all-to-all-start.3 = ((bf16[8,32,2]{1,2,0:T(2,128)(2,1)}), bf16[8,32,2]{1,2,0:T(2,128)(2,1)S(1)}, u32[]{:S(2)}, u32[]{:S(2)}) async-start(bf16[8,32,2]{1,2,0:T(2,128)(2,1)} %copy.43), calls=%async_computation.3 | async-start | bytes 8192 | tf_op jit(solution)/shard_map/all_to_all | solution.py:66
  110.8 0.2 fusion.2
  111.0 1.5 convolution_convert_fusion
  112.5 3.7 %all-to-all-done.3 = bf16[8,32,2]{1,2,0:T(2,128)(2,1)S(1)} async-done(((bf16[8,32,2]{1,2,0:T(2,128)(2,1)}), bf16[8,32,2]{1,2,0:T(2,128)(2,1)S(1)}, u32[]{:S(2)}, u32[]{:S(2)}) %all-to-all-start.3) | async-done | bytes 1056 | tf_op jit(solution)/shard_map/all_to_all | solution.py:66
  116.3 3.6 %all-to-all-start.4 = ((bf16[8,32,2048]{2,1,0:T(8,128)(2,1)}), bf16[8,32,2048]{2,1,0:T(8,128)(2,1)S(1)}, u32[]{:S(2)}, u32[]{:S(2)}) async-start(bf16[8,32,2048]{2,1,0:T(8,128)(2,1)} %bitcast.9), calls=%async_computation.4 | async-start | bytes 2097152 | tf_op jit(solution)/shard_map/all_to_all | solution.py:59
  119.8 0.1 copy.49
  120.0 0.3 mul.62
  120.3 0.2 copy.52
  120.5 4.7 %copy.47 = bf16[4,1,2,128,2048]{4,3,0,2,1:T(8,128)(2,1)} copy(bf16[4,1,2,128,2048]{4,3,2,1,0:T(8,128)(2,1)} %all-gather.8.cloned.1.call-done) | data formatting | bytes 8388608 | tf_op jit(solution)/shard_map/all_gather | solution.py:79
  125.3 21.0 %all-to-all-done.4 = bf16[8,32,2048]{2,1,0:T(8,128)(2,1)S(1)} async-done(((bf16[8,32,2048]{2,1,0:T(8,128)(2,1)}), bf16[8,32,2048]{2,1,0:T(8,128)(2,1)S(1)}, u32[]{:S(2)}, u32[]{:S(2)}) %all-to-all-start.4) | async-done | bytes 1048608 | tf_op jit(solution)/shard_map/all_to_all | solution.py:59
  146.3 3.6 %all-gather.4.cloned.1.call-done = bf16[1,2,512,2048]{3,2,1,0:T(8,128)(2,1)} async-done(((bf16[1,2,128,2048]{3,2,1,0:T(8,128)(2,1)}), bf16[1,2,512,2048]{3,2,1,0:T(8,128)(2,1)}) %all-gather.4.cloned.1.call-update) | async-done | bytes 4194320 | tf_op jit(solution)/shard_map/all_gather | solution.py:77
  149.9 4.4 %fusion.12 = f32[256,1024]{1,0:T(8,128)} fusion(bf16[256,2048]{1,0:T(8,128)(2,1)S(1)} %bitcast.51, bf16[1024,2048]{1,0:T(8,128)(2,1)} %bitcast.58), kind=kOutput, calls=%fused_computation.26 | convolution fusion | flops 1073741824 | bytes 6291456 | tf_op jit(solution)/shard_map/sd,hd->sh/dot_general | solution.py:18
  154.3 50.6 %all-gather.6.cloned.1.call-done = bf16[1,2,512,2048]{3,2,1,0:T(8,128)(2,1)} async-done(((bf16[1,2,128,2048]{3,2,1,0:T(8,128)(2,1)}), bf16[1,2,512,2048]{3,2,1,0:T(8,128)(2,1)}) %all-gather.6.cloned.1.call-update) | async-done | bytes 4194320 | tf_op jit(solution)/shard_map/all_gather | solution.py:78
  204.9 7.3 %convolution_convert_fusion.1 = bf16[256,2048]{1,0:T(8,128)(2,1)} fusion(bf16[1024,2048]{1,0:T(8,128)(2,1)} %bitcast.42, f32[256,1024]{1,0:T(8,128)S(1)} %bitcast.53, bf16[256,2048]{1,0:T(8,128)(2,1)S(1)} %bitcast.52, bf16[1024,2048]{1,0:T(8,128)(2,1)} %bitcast.59, f32[256,1024]{1,0:T(8,128)} %fusion.12), kind=kOutput, calls=%fused_computation.1 | convolution fusion | flops 2149842944 | bytes 12582912 | tf_op jit(solution)/shard_map/dot_general | solution.py:25
  212.2 4.6 %all-to-all-start.5 = ((bf16[8,32,2048]{2,1,0:T(8,128)(2,1)}), bf16[8,32,2048]{2,1,0:T(8,128)(2,1)S(1)}, u32[]{:S(2)}, u32[]{:S(2)}) async-start(bf16[8,32,2048]{2,1,0:T(8,128)(2,1)} %bitcast.54), calls=%async_computation.5 | async-start | bytes 2097152 | tf_op jit(solution)/shard_map/all_to_all | solution.py:83
  216.8 1.3 copy.48
  218.1 25.3 %all-to-all-done.5 = bf16[8,32,2048]{2,1,0:T(8,128)(2,1)S(1)} async-done(((bf16[8,32,2048]{2,1,0:T(8,128)(2,1)}), bf16[8,32,2048]{2,1,0:T(8,128)(2,1)S(1)}, u32[]{:S(2)}, u32[]{:S(2)}) %all-to-all-start.5) | async-done | bytes 1048608 | tf_op jit(solution)/shard_map/all_to_all | solution.py:83
  243.4 1.1 convolution_convert_fusion.2
  (19 shorter events, 0.3 us)
Async XLA Ops:
  7.2 99.5 %copy-start = (bf16[128,2]{0,1:T(2,128)(2,1)S(1)}, bf16[128,2]{0,1:T(2,128)(2,1)}, u32[]{:S(2)}) copy-start(bf16[128,2]{0,1:T(2,128)(2,1)} %param.13) | copy-start | bytes 1540
  7.2 113.4 %all-gather.8.cloned.1.call-start = ((), (), s32[]{:S(2)}) async-start(), calls=%async_computation.8 | async-start | bytes 5242880 | tf_op jit(solution)/shard_map/all_gather | solution.py:79
  9.1 34.2 %copy-start.3 = (f32[256]{0:T(256)S(1)}, f32[256]{0:T(256)}, u32[]{:S(2)}) copy-start(f32[256]{0:T(256)} %param.8) | copy-start | bytes 3076
  43.2 106.7 %all-gather.4.cloned.1.call-start = ((), (), s32[]{:S(2)}) async-start(), calls=%async_computation.6 | async-start | bytes 5242880 | tf_op jit(solution)/shard_map/all_gather | solution.py:77
  74.9 31.3 %copy-start.2 = (s32[128,1]{0,1:T(1,128)S(1)}, s32[128,1]{0,1:T(1,128)}, u32[]{:S(2)}) copy-start(s32[128,1]{0,1:T(1,128)} %param.12) | copy-start | bytes 1540
  74.9 35.9 %copy-start.1 = (bf16[128,2048]{1,0:T(8,128)(2,1)S(1)}, bf16[128,2048]{1,0:T(8,128)(2,1)}, u32[]{:S(2)}) copy-start(bf16[128,2048]{1,0:T(8,128)(2,1)} %param.7) | copy-start | bytes 1572868
  76.0 128.9 %all-gather.6.cloned.1.call-start = ((), (), s32[]{:S(2)}) async-start(), calls=%async_computation.7 | async-start | bytes 5242880 | tf_op jit(solution)/shard_map/all_gather | solution.py:78
  107.5 8.8 %all-to-all-start.3 = ((bf16[8,32,2]{1,2,0:T(2,128)(2,1)}), bf16[8,32,2]{1,2,0:T(2,128)(2,1)S(1)}, u32[]{:S(2)}, u32[]{:S(2)}) async-start(bf16[8,32,2]{1,2,0:T(2,128)(2,1)} %copy.43), calls=%async_computation.3 | async-start | bytes 8192 | tf_op jit(solution)/shard_map/all_to_all | solution.py:66
  116.3 30.1 %all-to-all-start.4 = ((bf16[8,32,2048]{2,1,0:T(8,128)(2,1)}), bf16[8,32,2048]{2,1,0:T(8,128)(2,1)S(1)}, u32[]{:S(2)}, u32[]{:S(2)}) async-start(bf16[8,32,2048]{2,1,0:T(8,128)(2,1)} %bitcast.9), calls=%async_computation.4 | async-start | bytes 2097152 | tf_op jit(solution)/shard_map/all_to_all | solution.py:59
  212.2 31.2 %all-to-all-start.5 = ((bf16[8,32,2048]{2,1,0:T(8,128)(2,1)}), bf16[8,32,2048]{2,1,0:T(8,128)(2,1)S(1)}, u32[]{:S(2)}, u32[]{:S(2)}) async-start(bf16[8,32,2048]{2,1,0:T(8,128)(2,1)} %bitcast.54), calls=%async_computation.5 | async-start | bytes 2097152 | tf_op jit(solution)/shard_map/all_to_all | solution.py:83
Sparse Core Ops, SparseCore 0:
  43.3 51.4 all-gather.7
  97.3 52.5 all-gather.3
  152.3 52.5 all-gather.5
